TPU v7x, 32 devices: a whole 2x2x4 slice. The times are simulated.
32 devices in a mesh: rep: 2 (over x), fs: 8 (over z, y), tp: 2 (over core).
Axes of the slice: x: 2, y: 2, z: 4, core: 2. Of those that a mesh axis runs over, the one named last changes fastest.
Arguments:
- tokens: bfloat16 [16384, 2048], P(('rep', 'fs'), 'tp'), may hold values from -6 to 6
- attention_pre_gain: float32 [2048], replicated, may hold values from 0.1 to 1.9
- query_matrix: bfloat16 [2048, 512], P('fs', 'tp'), may hold values from -0.125 to 0.125
- key_matrix: bfloat16 [2048, 512], P('fs', 'tp'), may hold values from -0.125 to 0.125
- value_matrix: bfloat16 [2048, 1024], P('fs', 'tp'), may hold values from -0.125 to 0.125
- decay_first_weight: bfloat16 [2048, 16], replicated, may hold values from -0.125 to 0.125
- decay_second_weight: bfloat16 [16, 512], P(None, 'tp'), may hold values from -1.5 to 1.5
- decay_offset_bias: float32 [512], P('tp'), may hold values from 0 to 6
- extra_log_surge: float32 [16384, 2], P(('rep', 'fs'), 'tp'), may hold values from -0.7 to 0
- readout_head_gain: float32 [512], replicated, may hold values from 0.1 to 1.9
- output_matrix: bfloat16 [1024, 2048], P('tp', 'fs'), may hold values from -2.4375 to 2.4375
- attention_post_gain: float32 [2048], P('tp'), may hold values from 0.1 to 1.9
- feedforward_pre_gain: float32 [2048], replicated, may hold values from 0.1 to 1.9
- up_matrix: bfloat16 [2048, 4096], P('fs', 'tp'), may hold values from -0.125 to 0.125
- down_matrix: bfloat16 [4096, 2048], P('tp', 'fs'), may hold values from -1.21875 to 1.21875
- feedforward_post_gain: float32 [2048], P('tp'), may hold values from 0.1 to 1.9
Outputs:
- layer_out: bfloat16 [16384, 2048], P(('rep', 'fs'), 'tp')
All inputs are finite; a program needn't handle non-finite values.
Results may differ from a plain program's by a relative error of at most 0.017.
Values may be sent and summed in bfloat16 or wider, within the bound.
A program may use at most 128 MiB of HBM per device.

v0:
```python
import jax
import jax.numpy as jnp
from jax import lax
from jax.sharding import PartitionSpec as P

KEY_WIDTH = 256
DV = 512
BLOCK = 64
EPS = 1e-06


def pre_norm(rows, gain):
    values = rows.astype(jnp.float32)
    scale = lax.rsqrt(jnp.mean(values * values, axis=-1, keepdims=True) + EPS)
    return (values * scale * gain).astype(jnp.bfloat16)


def block_attention(queries, keys_in, values_in, log_gates):
    head_count, token_length, key_size = queries.shape
    value_size = values_in.shape[-1]
    blocks = token_length // BLOCK

    def to_blocks(array):
        return array.reshape(head_count, blocks, BLOCK, array.shape[-1]).transpose(1, 0, 2, 3)

    causal = jnp.tril(jnp.ones((BLOCK, BLOCK), dtype=bool))[None, :, :, None]
    highest = lax.Precision.HIGHEST

    def advance(memory_state, inputs):
        query_blk, key_blk, value_blk, gate_blk = inputs
        cumulative = jnp.cumsum(gate_blk, axis=1)
        carried = jnp.einsum(
            "hid,hde->hie", query_blk * jnp.exp(cumulative), memory_state, precision=highest
        )
        spread_log = cumulative[:, :, None, :] - cumulative[:, None, :, :]
        weights = jnp.exp(jnp.where(causal, spread_log, -jnp.inf))
        scores = jnp.einsum("hid,hjd,hijd->hij", query_blk, key_blk, weights, precision=highest)
        readout = carried + jnp.einsum("hij,hje->hie", scores, value_blk, precision=highest)
        final_log = cumulative[:, -1:, :]
        memory_state = jnp.exp(final_log[:, 0, :])[:, :, None] * memory_state + jnp.einsum(
            "hjd,hje->hde", key_blk * jnp.exp(final_log - cumulative), value_blk, precision=highest
        )
        return (memory_state, readout)

    start_state = jnp.zeros((head_count, key_size, value_size), jnp.float32)
    _, readout = lax.scan(
        advance,
        start_state,
        (to_blocks(queries), to_blocks(keys_in), to_blocks(values_in), to_blocks(log_gates)),
    )
    return readout.transpose(1, 0, 2, 3).reshape(head_count, token_length, value_size)


def make_adder(left):

    def add_rows(total, piece, start):
        return jnp.dot(left, piece, preferred_element_type=jnp.float32)

    return add_rows


def make_projector(left, piece):
    return jnp.dot(left, piece, preferred_element_type=jnp.float32)


def on_device(
    tokens,
    attention_pre_gain,
    query_matrix,
    key_matrix,
    value_matrix,
    decay_first_weight,
    decay_second_weight,
    decay_offset_bias,
    extra_log_surge,
    readout_head_gain,
    output_matrix,
    attention_post_gain,
    feedforward_pre_gain,
    up_matrix,
    down_matrix,
    feedforward_post_gain,
):
    token_length = tokens.shape[0]
    gathered = lax.all_gather(tokens, "tp", axis=1, tiled=True)
    width = gathered.shape[1]
    normed = pre_norm(gathered, attention_pre_gain)
    add_rows = make_adder(normed)
    key_cols = query_matrix.shape[1]
    value_cols = value_matrix.shape[1]
    empty_key = jnp.zeros((token_length, key_cols), jnp.float32)
    empty_value = jnp.zeros((token_length, value_cols), jnp.float32)
    start = jnp.int32(0)
    query_proj = add_rows(empty_key, lax.all_gather(query_matrix, "fs", axis=0, tiled=True), start)
    key_proj = add_rows(empty_key, lax.all_gather(key_matrix, "fs", axis=0, tiled=True), start)
    value_proj = add_rows(
        empty_value, lax.all_gather(value_matrix, "fs", axis=0, tiled=True), start
    )
    query_proj = query_proj.astype(jnp.bfloat16)
    key_proj = key_proj.astype(jnp.bfloat16)
    value_proj = value_proj.astype(jnp.bfloat16)
    rank_rows = jnp.dot(normed, decay_first_weight, preferred_element_type=jnp.float32).astype(
        jnp.bfloat16
    )
    gate_source_input = (
        jnp.dot(rank_rows, decay_second_weight, preferred_element_type=jnp.float32)
        + decay_offset_bias
    )
    head_count = key_cols // KEY_WIDTH
    logarithm_decay = (jax.nn.log_sigmoid(gate_source_input) / 16.0).reshape(
        token_length, head_count, KEY_WIDTH
    ) + extra_log_surge[:, :, None]

    def by_head(array, size):
        return array.astype(jnp.float32).reshape(token_length, head_count, size).transpose(1, 0, 2)

    queries = by_head(query_proj, KEY_WIDTH) * KEY_WIDTH ** (-0.5)
    readout = block_attention(
        queries,
        by_head(key_proj, KEY_WIDTH),
        by_head(value_proj, DV),
        logarithm_decay.transpose(1, 0, 2),
    )
    readout = readout.transpose(1, 0, 2)
    head_scale = lax.rsqrt(jnp.mean(readout * readout, axis=-1, keepdims=True) + EPS)
    mixed = (
        (readout * head_scale * readout_head_gain)
        .astype(jnp.bfloat16)
        .reshape(token_length, value_cols)
    )
    partial_attn = make_projector(mixed, lax.all_gather(output_matrix, "fs", axis=1, tiled=True))
    attn = lax.psum_scatter(
        partial_attn.astype(jnp.bfloat16), "tp", scatter_dimension=1, tiled=True
    ).astype(jnp.float32)
    attn_total = lax.psum(jnp.sum(attn * attn, axis=1), "tp")
    attn_scale = lax.rsqrt(attn_total / width + EPS)[:, None]
    resid = (tokens.astype(jnp.float32) + attn * attn_scale * attention_post_gain).astype(
        jnp.bfloat16
    )
    gathered_mid = lax.all_gather(resid, "tp", axis=1, tiled=True)
    normed_mid = pre_norm(gathered_mid, feedforward_pre_gain)
    whole_up = lax.all_gather(up_matrix, "fs", axis=0, tiled=True)
    hidden = jnp.dot(normed_mid, whole_up, preferred_element_type=jnp.float32)
    hidden = jax.nn.relu(hidden)
    squared = (hidden * hidden).astype(jnp.bfloat16)
    partial_feed = make_projector(squared, lax.all_gather(down_matrix, "fs", axis=1, tiled=True))
    feed = lax.psum_scatter(
        partial_feed.astype(jnp.bfloat16), "tp", scatter_dimension=1, tiled=True
    ).astype(jnp.float32)
    feed_total = lax.psum(jnp.sum(feed * feed, axis=1), "tp")
    feed_scale = lax.rsqrt(feed_total / width + EPS)[:, None]
    return (resid.astype(jnp.float32) + feed * feed_scale * feedforward_post_gain).astype(
        jnp.bfloat16
    )


def solution(mesh):
    return jax.shard_map(
        on_device,
        mesh=mesh,
        in_specs=(
            P(("rep", "fs"), "tp"),
            P(),
            P("fs", "tp"),
            P("fs", "tp"),
            P("fs", "tp"),
            P(),
            P(None, "tp"),
            P("tp"),
            P(("rep", "fs"), "tp"),
            P(),
            P("tp", "fs"),
            P("tp"),
            P(),
            P("fs", "tp"),
            P("tp", "fs"),
            P("tp"),
        ),
        out_specs=P(("rep", "fs"), "tp"),
        check_vma=False,
    )
```

profile of v0, /device:TPU:0, one launch (start us, length us, event | category | flops | bytes accessed | tf_op | source)
XLA Modules:
  0.0 660.1 jit_solution(7252431059757820232)
XLA Ops:
  10.0 15.3 %all-gather.9.cloned.1.call-done = bf16[1024,2048]{1,0:T(8,128)(2,1)} async-done(((bf16[1024,1024]{1,0:T(8,128)(2,1)}), bf16[1024,2048]{1,0:T(8,128)(2,1)}) %all-gather.9.cloned.1.call-update) | async-done | bytes 4194320 | tf_op jit(solution)/shard_map/all_gather | solution.py:85
  25.3 3.2 fusion.30
  28.8 3.0 fusion.32
  31.7 46.0 %all-gather.13.cloned.1.call-done = bf16[2048,512]{1,0:T(8,128)(2,1)} async-done(((bf16[256,512]{1,0:T(8,128)(2,1)}), bf16[2048,512]{1,0:T(8,128)(2,1)}) %all-gather.13.cloned.1.call-update) | async-done | bytes 2097168 | tf_op jit(solution)/shard_map/all_gather | solution.py:97
  77.7 5.2 convolution_convert_fusion.1
  82.9 1.6 convert.5
  84.5 34.2 %all-gather.11.cloned.1.call-done = bf16[2048,256]{1,0:T(8,128)(2,1)} async-done(((bf16[256,256]{1,0:T(8,128)(2,1)}), bf16[2048,256]{1,0:T(8,128)(2,1)}) %all-gather.11.cloned.1.call-update) | async-done | bytes 1048592 | tf_op jit(solution)/shard_map/all_gather | solution.py:95
  118.7 3.7 convolution_convert_fusion.3
  123.6 5.1 fusion.63
  128.7 31.0 %all-gather.15.cloned.1.call-done = bf16[2048,256]{1,0:T(8,128)(2,1)} async-done(((bf16[256,256]{1,0:T(8,128)(2,1)}), bf16[2048,256]{1,0:T(8,128)(2,1)}) %all-gather.15.cloned.1.call-update) | async-done | bytes 1048592 | tf_op jit(solution)/shard_map/all_gather | solution.py:94
  159.7 4.8 fusion.60
  164.5 150.9 %while.13 = (s32[]{:T(128)}, f32[1,256,512]{2,1,0:T(8,128)S(1)}, f32[16,1,64,512]{3,2,1,0:T(8,128)S(1)}, f32[16,1,64,256]{3,2,1,0:T(8,128)}, f32[16,1,64,256]{3,...) while((s32[]{:T(128)}, f32[1,256,512]{2,1,0:T(8,128)S(1)}, ...), condition=%wide.region_3.4_spmd.clone, body=%wide.region_1.3_spmd.clone.sunk | while | flops 233373696 | bytes 11649660 | solution.py:46
  167.2 2.5 fusion.98
  172.3 1.6 fusion.96
  176.6 2.5 fusion.98
  181.7 1.6 fusion.96
  186.1 2.5 fusion.98
  189.8 1.3 fusion.100
  191.1 1.6 fusion.96
  195.5 2.5 fusion.98
  200.6 1.6 fusion.96
  204.9 2.5 fusion.98
  210.0 1.6 fusion.96
  214.4 2.5 fusion.98
  219.4 1.6 fusion.96
  223.8 2.5 fusion.98
  228.9 1.6 fusion.96
  233.2 2.5 fusion.98
  238.3 1.6 fusion.96
  242.7 2.5 fusion.98
  246.4 1.3 fusion.100
  247.7 1.6 fusion.96
  252.1 2.5 fusion.98
  255.8 1.3 fusion.100
  257.2 1.6 fusion.96
  261.5 2.5 fusion.98
  265.3 1.3 fusion.100
  266.6 1.6 fusion.96
  270.9 2.5 fusion.98
  274.7 1.3 fusion.100
  276.0 1.6 fusion.96
  280.4 2.5 fusion.98
  284.1 1.3 fusion.100
  285.4 1.6 fusion.96
  289.8 2.5 fusion.98
  294.9 1.6 fusion.96
  299.2 2.5 fusion.98
  304.3 1.6 fusion.96
  308.7 2.5 fusion.98
  313.7 1.6 fusion.96
  316.0 5.9 convolution_convert_fusion
  322.0 10.7 %reduce-scatter.3.cloned.1.call-done = bf16[1024,1024]{1,0:T(8,128)(2,1)} async-done(((bf16[1024,2048]{1,0:T(8,128)(2,1)}), bf16[1024,1024]{1,0:T(8,128)(2,1)}) %reduce-scatter.3.cloned.1.call-update) | async-done | bytes 2097168 | tf_op jit(solution)/shard_map/reduce_scatter | solution.py:132
  332.6 2.1 fusion.36
  334.7 2.5 psum.14
  337.2 3.7 fusion.39
  342.5 13.6 %all-gather.19.cloned.1.call-done = bf16[1024,2048]{1,0:T(8,128)(2,1)} async-done(((bf16[1024,1024]{1,0:T(8,128)(2,1)}), bf16[1024,2048]{1,0:T(8,128)(2,1)}) %all-gather.19.cloned.1.call-update) | async-done | bytes 4194320 | tf_op jit(solution)/shard_map/all_gather | solution.py:140
  356.1 3.1 fusion.33
  359.2 124.7 %all-gather.21.cloned.1.call-done = bf16[2048,2048]{1,0:T(8,128)(2,1)} async-done(((bf16[256,2048]{1,0:T(8,128)(2,1)}), bf16[2048,2048]{1,0:T(8,128)(2,1)}) %all-gather.21.cloned.1.call-update) | async-done | bytes 8388624 | tf_op jit(solution)/shard_map/all_gather | solution.py:142
  483.9 125.2 %all-gather.23.cloned.1.call-done = bf16[2048,2048]{1,0:T(8,128)(2,1)} async-done(((bf16[2048,256]{1,0:T(8,128)(2,1)}), bf16[2048,2048]{1,0:T(8,128)(2,1)}) %all-gather.23.cloned.1.call-update) | async-done | bytes 8388624 | tf_op jit(solution)/shard_map/all_gather | solution.py:146
  609.1 25.6 %fusion.53 = bf16[1024,2048]{1,0:T(8,128)(2,1)} fusion(bf16[2048,2048]{1,0:T(8,128)(2,1)} %all-gather.23.cloned.1.call-done, bf16[2048,2048]{1,0:T(8,128)(2,1)} %all-gather.21.cloned.1.call-done, bf16[1024,2048]{1,0:T(8,128)(2,1)} %all-gather.19.cloned.1.call-done, f32[2048]{0:T(1024)S(1)} %copy-done.10, f32[1024]{0:T(1024)S(1)} %add_rsqrt_fusion.2), kind=kOutput, calls=%fused_computation.65 | convolution fusion | flops 17196646400 | bytes 25178112 | tf_op jit(solution)/shard_map/dot_general | solution.py:63
  634.7 10.2 %reduce-scatter.5.cloned.1.call-done = bf16[1024,1024]{1,0:T(8,128)(2,1)} async-done(((bf16[1024,2048]{1,0:T(8,128)(2,1)}), bf16[1024,1024]{1,0:T(8,128)(2,1)}) %reduce-scatter.5.cloned.1.call-update) | async-done | bytes 2097168 | tf_op jit(solution)/shard_map/reduce_scatter | solution.py:147
  644.9 2.1 fusion.40
  647.0 2.5 psum.15
  649.5 3.7 fusion.43
  (196 shorter events, 82.5 us)
Async XLA Ops:
  6.5 117.0 %copy-start = (bf16[2048,16]{0,1:T(8,128)(2,1)S(1)}, bf16[2048,16]{0,1:T(8,128)(2,1)}, u32[]{:S(2)}) copy-start(bf16[2048,16]{0,1:T(8,128)(2,1)} %param.23) | copy-start | bytes 196612
  6.5 22.0 %copy-start.5 = (f32[2048]{0:T(1024)S(1)}, f32[2048]{0:T(1024)}, u32[]{:S(2)}) copy-start(f32[2048]{0:T(1024)} %param.19) | copy-start | bytes 24580
  6.5 18.8 %all-gather.9.cloned.1.call-start = ((), (), s32[]{:S(2)}) async-start(), calls=%async_computation.2 | async-start | bytes 6291456 | tf_op jit(solution)/shard_map/all_gather | solution.py:85
  7.3 70.5 %all-gather.13.cloned.1.call-start = ((), (), s32[]{:S(2)}) async-start(), calls=%async_computation.4 | async-start | bytes 2359296 | tf_op jit(solution)/shard_map/all_gather | solution.py:97
  8.0 110.7 %all-gather.11.cloned.1.call-start = ((), (), s32[]{:S(2)}) async-start(), calls=%async_computation.3 | async-start | bytes 1179648 | tf_op jit(solution)/shard_map/all_gather | solution.py:95
  8.7 151.0 %all-gather.15.cloned.1.call-start = ((), (), s32[]{:S(2)}) async-start(), calls=%async_computation.5 | async-start | bytes 1179648 | tf_op jit(solution)/shard_map/all_gather | solution.py:94
  9.3 306.7 %all-gather.17.cloned.1.call-start = ((), (), s32[]{:S(2)}) async-start(), calls=%async_computation.6 | async-start | bytes 2359296 | tf_op jit(solution)/shard_map/all_gather | solution.py:131
  9.9 322.7 %reduce-scatter.3.cloned.1.call-start = ((), (), s32[]{:S(2)}) async-start(), calls=%async_computation.7 | async-start | bytes 6291456 | tf_op jit(solution)/shard_map/reduce_scatter | solution.py:132
  25.3 3.4 copy-start.3
  84.5 39.0 %copy-start.9 = (bf16[16,256]{1,0:T(8,128)(2,1)S(1)}, bf16[16,256]{1,0:T(8,128)(2,1)}, u32[]{:S(2)}) copy-start(bf16[16,256]{1,0:T(8,128)(2,1)} %param.24) | copy-start | bytes 24580
  84.5 39.0 %copy-start.11 = (f32[1024,1]{0,1:T(1,128)S(1)}, f32[1024,1]{0,1:T(1,128)}, u32[]{:S(2)}) copy-start(f32[1024,1]{0,1:T(1,128)} %param.26) | copy-start | bytes 12292
  84.5 39.0 %copy-start.12 = (f32[256]{0:T(256)S(1)}, f32[256]{0:T(256)}, u32[]{:S(2)}) copy-start(f32[256]{0:T(256)} %param.25) | copy-start | bytes 3076
  164.5 151.2 %copy-start.8 = (f32[512]{0:T(512)S(1)}, f32[512]{0:T(512)}, u32[]{:S(2)}) copy-start(f32[512]{0:T(512)} %param.27) | copy-start | bytes 6148
  321.9 15.3 %copy-start.4 = (bf16[1024,1024]{1,0:T(8,128)(2,1)S(1)}, bf16[1024,1024]{1,0:T(8,128)(2,1)}, u32[]{:S(2)}) copy-start(bf16[1024,1024]{1,0:T(8,128)(2,1)} %param.18) | copy-start | bytes 6291460
  321.9 15.3 %copy-start.6 = (f32[1024]{0:T(1024)S(1)}, f32[1024]{0:T(1024)}, u32[]{:S(2)}) copy-start(f32[1024]{0:T(1024)} %param.29) | copy-start | bytes 12292
  321.9 34.2 %all-gather.19.cloned.1.call-start = ((), (), s32[]{:S(2)}) async-start(), calls=%async_computation.8 | async-start | bytes 6291456 | tf_op jit(solution)/shard_map/all_gather | solution.py:140
  340.9 268.2 %copy-start.10 = (f32[2048]{0:T(1024)S(1)}, f32[2048]{0:T(1024)}, u32[]{:S(2)}) copy-start(f32[2048]{0:T(1024)} %param.30) | copy-start | bytes 24580
  341.0 142.9 %all-gather.21.cloned.1.call-start = ((), (), s32[]{:S(2)}) async-start(), calls=%async_computation.9 | async-start | bytes 9437184 | tf_op jit(solution)/shard_map/all_gather | solution.py:142
  341.7 267.4 %all-gather.23.cloned.1.call-start = ((), (), s32[]{:S(2)}) async-start(), calls=%async_computation.10 | async-start | bytes 9437184 | tf_op jit(solution)/shard_map/all_gather | solution.py:146
  342.4 302.5 %reduce-scatter.5.cloned.1.call-start = ((), (), s32[]{:S(2)}) async-start(), calls=%async_computation.11 | async-start | bytes 6291456 | tf_op jit(solution)/shard_map/reduce_scatter | solution.py:147
  634.7 14.8 %copy-start.2 = (bf16[1024,1024]{1,0:T(8,128)(2,1)S(1)}, bf16[1024,1024]{1,0:T(8,128)(2,1)}, u32[]{:S(2)}) copy-start(bf16[1024,1024]{1,0:T(8,128)(2,1)} %fusion.39) | copy-start | bytes 6291460
  634.7 14.8 %copy-start.7 = (f32[1024]{0:T(1024)S(1)}, f32[1024]{0:T(1024)}, u32[]{:S(2)}) copy-start(f32[1024]{0:T(1024)} %param.33) | copy-start | bytes 12292
  634.7 18.5 %copy-start.1 = (bf16[2048,16]{0,1:T(8,128)(2,1)S(1)}, bf16[2048,16]{0,1:T(8,128)(2,1)}, u32[]{:S(2)}) copy-start(bf16[2048,16]{0,1:T(8,128)(2,1)} %param.23) | copy-start | bytes 196612
Sparse Core Ops, SparseCore 0:
  8.9 16.3 all-gather.8
  27.4 50.2 all-gather.12
  79.8 38.7 all-gather.10
  120.7 38.9 all-gather.14
  161.6 49.1 all-gather.16
  322.0 10.5 reduce-scatter.2
  341.1 14.9 all-gather.18
  358.2 125.6 all-gather.20
  485.9 123.1 all-gather.22
  634.9 10.0 reduce-scatter.4
where the time goes:
time: 663 us; the launch traced here: 660 us
  waiting for transfers between devices  415 us (63%)
  matrix products  117 us (18%)
  other arithmetic  79.4 us (12%)
  local copies, waits for them, and re-layouts  28.2 us (4%)
  between operations  13.7 us (2%)
    all_gather x1, waiting for transfers between devices, on_device(): lax.all_gather(down_matrix, 'fs', axis=1, tiled=True)  125 us
    all_gather x1, waiting for transfers between devices, on_device(): whole_up = lax.all_gather(up_matrix, 'fs', axis=0, tiled=True)  125 us
    all_gather x1, waiting for transfers between devices, on_device(): lax.all_gather(value_matrix, 'fs', axis=0, tiled=True)  46 us
    dot_general x16, other arithmetic, advance(): jnp.einsum('hid,hjd,hijd->hij', query_blk, key_blk, weights, precision=hi...  40.2 us
    all_gather x1, waiting for transfers between devices, on_device(): lax.all_gather(key_matrix, 'fs', axis=0, tiled=True)  34.2 us
    dot_general x2, matrix products, make_projector(): return jnp.dot(left, piece, preferred_element_type=jnp.float32)  31.5 us
    all_gather x1, waiting for transfers between devices, on_device(): lax.all_gather(query_matrix, 'fs', axis=0, tiled=True)  31 us
    dot_general x16, matrix products, advance(): jnp.einsum('hjd,hje->hde', key_blk * jnp.exp(final_log - cumulative), val...  26.3 us
  transfers between devices with their start and end apart: 10, of which 9 were waited for; matrix products, arithmetic and copies ran while one was open for 27% of the time, Pallas kernels for 0%

commit v1 on v0

--- a/solution.py
+++ b/solution.py
@@ -7,6 +7,17 @@
 DV = 512
 BLOCK = 64
 EPS = 1e-06
+
+
+def gather_by_hops(x, mesh_axis, d):
+    peers = lax.axis_size(mesh_axis)
+    right = [(i, (i + 1) % peers) for i in range(peers)]
+    pieces = [x]
+    for reach in range(1, peers):
+        pieces = [lax.ppermute(pieces[0], mesh_axis, right), *pieces]
+    whole = jnp.concatenate(pieces, axis=d)
+    shift = (lax.axis_index(mesh_axis) + 1) * pieces[-1].shape[d]
+    return jnp.roll(whole, shift, axis=d)
 
 
 def pre_norm(rows, gain):
@@ -139,7 +150,7 @@
     )
     gathered_mid = lax.all_gather(resid, "tp", axis=1, tiled=True)
     normed_mid = pre_norm(gathered_mid, feedforward_pre_gain)
-    whole_up = lax.all_gather(up_matrix, "fs", axis=0, tiled=True)
+    whole_up = gather_by_hops(up_matrix, "fs", 0)
     hidden = jnp.dot(normed_mid, whole_up, preferred_element_type=jnp.float32)
     hidden = jax.nn.relu(hidden)
     squared = (hidden * hidden).astype(jnp.bfloat16)

time: 663 us -> 695 us (1.048)
  local copies, waits for them, and re-layouts: 28.2 us -> 53.3 us
    ppermute x0 -> x7, waiting for transfers between devices: none -> 267 us  [gather_by_hops(): pieces = [lax.ppermute(pieces[0], mesh_axis, right), *pieces]]
    all_gather x1, waiting for transfers between devices: 125 us -> 0.02 us  [on_device(): lax.all_gather(down_matrix, 'fs', axis=1, tiled=True)]
    all_gather x1 -> x0, waiting for transfers between devices: 125 us -> none  [on_device(): whole_up = lax.all_gather(up_matrix, 'fs', axis=0, tiled=True)]
    unnamed x26 -> x55, local copies, waits for them, and re-layouts: 0.25 us -> 24.3 us
    all_gather x1, waiting for transfers between devices: 13.6 us -> 0.01 us  [on_device(): gathered_mid = lax.all_gather(resid, 'tp', axis=1, tiled=True)]
  transfers between devices with their start and end apart: 10 -> 16, of which waited for: 9 -> 13; matrix products, arithmetic and copies ran while one was open for 27% -> 29% of each run, Pallas kernels for 0% -> 0%
where the time goes in v1:
time: 695 us; the launch traced here: 692 us
  waiting for transfers between devices  420 us (60%)
  matrix products  117 us (17%)
  other arithmetic  79.5 us (11%)
  local copies, waits for them, and re-layouts  53.3 us (8%)
  between operations  13.4 us (2%)
    ppermute x7, waiting for transfers between devices, gather_by_hops(): pieces = [lax.ppermute(pieces[0], mesh_axis, right), *pieces]  267 us
    all_gather x1, waiting for transfers between devices, on_device(): lax.all_gather(value_matrix, 'fs', axis=0, tiled=True)  46 us
    dot_general x16, other arithmetic, advance(): jnp.einsum('hid,hjd,hijd->hij', query_blk, key_blk, weights, precision=hi...  40.2 us
    all_gather x1, waiting for transfers between devices, on_device(): lax.all_gather(key_matrix, 'fs', axis=0, tiled=True)  34.2 us
    dot_general x2, matrix products, make_projector(): return jnp.dot(left, piece, preferred_element_type=jnp.float32)  31.7 us
    all_gather x1, waiting for transfers between devices, on_device(): lax.all_gather(query_matrix, 'fs', axis=0, tiled=True)  31 us
    dot_general x16, matrix products, advance(): jnp.einsum('hjd,hje->hde', key_blk * jnp.exp(final_log - cumulative), val...  26.3 us
    unnamed x55, local copies, waits for them, and re-layouts  24.3 us
  transfers between devices with their start and end apart: 16, of which 13 were waited for; matrix products, arithmetic and copies ran while one was open for 29% of the time, Pallas kernels for 0%

profile of v1, /device:TPU:0, one launch (start us, length us, event | category | flops | bytes accessed | tf_op | source)
XLA Modules:
  0.0 691.7 jit_solution(15321990995125744202)
XLA Ops:
  10.0 15.3 %all-gather.8.cloned.1.call-done = bf16[1024,2048]{1,0:T(8,128)(2,1)} async-done(((bf16[1024,1024]{1,0:T(8,128)(2,1)}), bf16[1024,2048]{1,0:T(8,128)(2,1)}) %all-gather.8.cloned.1.call-update) | async-done | bytes 4194320 | tf_op jit(solution)/shard_map/all_gather | solution.py:96
  25.3 3.2 fusion.30
  28.8 3.0 fusion.32
  31.7 46.0 %all-gather.12.cloned.1.call-done = bf16[2048,512]{1,0:T(8,128)(2,1)} async-done(((bf16[256,512]{1,0:T(8,128)(2,1)}), bf16[2048,512]{1,0:T(8,128)(2,1)}) %all-gather.12.cloned.1.call-update) | async-done | bytes 2097168 | tf_op jit(solution)/shard_map/all_gather | solution.py:108
  77.7 5.2 convolution_convert_fusion.1
  84.5 34.2 %all-gather.10.cloned.1.call-done = bf16[2048,256]{1,0:T(8,128)(2,1)} async-done(((bf16[256,256]{1,0:T(8,128)(2,1)}), bf16[2048,256]{1,0:T(8,128)(2,1)}) %all-gather.10.cloned.1.call-update) | async-done | bytes 1048592 | tf_op jit(solution)/shard_map/all_gather | solution.py:106
  118.7 3.7 convolution_convert_fusion.3
  123.6 5.1 fusion.70
  128.7 31.0 %all-gather.14.cloned.1.call-done = bf16[2048,256]{1,0:T(8,128)(2,1)} async-done(((bf16[256,256]{1,0:T(8,128)(2,1)}), bf16[2048,256]{1,0:T(8,128)(2,1)}) %all-gather.14.cloned.1.call-update) | async-done | bytes 1048592 | tf_op jit(solution)/shard_map/all_gather | solution.py:105
  159.7 4.8 fusion.67
  164.5 150.9 %while.13 = (s32[]{:T(128)}, f32[1,256,512]{2,1,0:T(8,128)S(1)}, f32[16,1,64,512]{3,2,1,0:T(8,128)S(1)}, f32[16,1,64,256]{3,2,1,0:T(8,128)}, f32[16,1,64,256]{3,...) while((s32[]{:T(128)}, f32[1,256,512]{2,1,0:T(8,128)S(1)}, ...), condition=%wide.region_3.4_spmd.clone, body=%wide.region_1.3_spmd.clone.sunk | while | flops 233373696 | bytes 11649660 | solution.py:57
  167.2 2.5 fusion.106
  176.6 2.5 fusion.106
  181.7 1.6 fusion.104
  186.1 2.5 fusion.106
  191.1 1.6 fusion.104
  195.5 2.5 fusion.106
  200.6 1.6 fusion.104
  204.9 2.5 fusion.106
  210.0 1.6 fusion.104
  214.4 2.5 fusion.106
  219.4 1.6 fusion.104
  223.8 2.5 fusion.106
  228.9 1.6 fusion.104
  233.2 2.5 fusion.106
  238.3 1.6 fusion.104
  242.7 2.5 fusion.106
  247.7 1.6 fusion.104
  252.1 2.5 fusion.106
  257.2 1.6 fusion.104
  261.5 2.5 fusion.106
  266.6 1.6 fusion.104
  270.9 2.5 fusion.106
  276.0 1.6 fusion.104
  280.4 2.5 fusion.106
  285.4 1.6 fusion.104
  289.8 2.5 fusion.106
  294.9 1.6 fusion.104
  299.2 2.5 fusion.106
  304.3 1.6 fusion.104
  308.7 2.5 fusion.106
  316.0 5.9 convolution_convert_fusion
  321.9 10.7 %reduce-scatter.3.cloned.1.call-done = bf16[1024,1024]{1,0:T(8,128)(2,1)} async-done(((bf16[1024,2048]{1,0:T(8,128)(2,1)}), bf16[1024,1024]{1,0:T(8,128)(2,1)}) %reduce-scatter.3.cloned.1.call-update) | async-done | bytes 2097168 | tf_op jit(solution)/shard_map/reduce_scatter | solution.py:143
  332.6 2.1 fusion.38
  334.7 2.5 psum.14
  337.2 3.8 fusion.41
  341.8 1.9 collective-permute-start
  343.7 26.3 %collective-permute-done = bf16[256,2048]{1,0:T(8,128)(2,1)S(1)} collective-permute-done((bf16[256,2048]{1,0:T(8,128)(2,1)S(1)}, bf16[256,2048]{1,0:T(8,128)(2,1)S(1)}, u32[]{:S(2)}, u32[]{:S(2)}) %collective-permute-start) | collective-permute-done | bytes 1048608 | tf_op jit(solution)/shard_map/ppermute | solution.py:17
  370.0 48.4 %collective-permute-done.1 = bf16[256,2048]{1,0:T(8,128)(2,1)S(1)} collective-permute-done((bf16[256,2048]{1,0:T(8,128)(2,1)S(1)}, bf16[256,2048]{1,0:T(8,128)(2,1)S(1)}, u32[]{:S(2)}, u32[]{:S(2)}) %collective-permute-start.1) | collective-permute-done | bytes 1048608 | tf_op jit(solution)/shard_map/ppermute | solution.py:17
  418.4 42.5 %collective-permute-done.2 = bf16[256,2048]{1,0:T(8,128)(2,1)S(1)} collective-permute-done((bf16[256,2048]{1,0:T(8,128)(2,1)S(1)}, bf16[256,2048]{1,0:T(8,128)(2,1)S(1)}, u32[]{:S(2)}, u32[]{:S(2)}) %collective-permute-start.2) | collective-permute-done | bytes 1048608 | tf_op jit(solution)/shard_map/ppermute | solution.py:17
  461.9 50.2 %collective-permute-done.3 = bf16[256,2048]{1,0:T(8,128)(2,1)S(1)} collective-permute-done((bf16[256,2048]{1,0:T(8,128)(2,1)S(1)}, bf16[256,2048]{1,0:T(8,128)(2,1)S(1)}, u32[]{:S(2)}, u32[]{:S(2)}) %collective-permute-start.3) | collective-permute-done | bytes 1048608 | tf_op jit(solution)/shard_map/ppermute | solution.py:17
  513.0 49.9 %collective-permute-done.4 = bf16[256,2048]{1,0:T(8,128)(2,1)S(1)} collective-permute-done((bf16[256,2048]{1,0:T(8,128)(2,1)S(1)}, bf16[256,2048]{1,0:T(8,128)(2,1)S(1)}, u32[]{:S(2)}, u32[]{:S(2)}) %collective-permute-start.4) | collective-permute-done | bytes 1048608 | tf_op jit(solution)/shard_map/ppermute | solution.py:17
  564.0 24.2 %collective-permute-done.5 = bf16[256,2048]{1,0:T(8,128)(2,1)} collective-permute-done((bf16[256,2048]{1,0:T(8,128)(2,1)S(1)}, bf16[256,2048]{1,0:T(8,128)(2,1)}, u32[]{:S(2)}, u32[]{:S(2)}) %collective-permute-start.5) | collective-permute-done | bytes 1048608 | tf_op jit(solution)/shard_map/ppermute | solution.py:17
  588.2 25.2 %collective-permute-done.6 = bf16[256,2048]{1,0:T(8,128)(2,1)} collective-permute-done((bf16[256,2048]{1,0:T(8,128)(2,1)}, bf16[256,2048]{1,0:T(8,128)(2,1)}, u32[]{:S(2)}, u32[]{:S(2)}) %collective-permute-start.6) | collective-permute-done | bytes 1048608 | tf_op jit(solution)/shard_map/ppermute | solution.py:17
  613.4 2.3 constant_dynamic-update-slice_fusion.15
  615.7 2.3 constant_dynamic-update-slice_fusion.14
  624.4 2.4 constant_dynamic-update-slice_fusion.7
  626.8 2.3 constant_dynamic-update-slice_fusion.6
  635.5 3.1 fusion.33
  638.6 25.9 %fusion.58 = bf16[1024,2048]{1,0:T(8,128)(2,1)} fusion(bf16[2048,2048]{1,0:T(8,128)(2,1)} %all-gather.20.cloned.1.call-done, bf16[4096,2048]{1,0:T(8,128)(2,1)} %constant_dynamic-update-slice_fusion, s32[]{:T(128)S(6)} %select_n.29, bf16[1024,2048]{1,0:T(8,128)(2,1)} %all-gather.18.cloned.1.call-done, f32[2048]{0:T(1024)S(1)} %copy-done.17, ...), kind=kOutput, calls=%fused_computation.67 | convolution fusion | flops 17196646400 | bytes 25178116 | tf_op jit(solution)/shard_map/dot_general | solution.py:74
  664.5 12.4 %reduce-scatter.5.cloned.1.call-done = bf16[1024,1024]{1,0:T(8,128)(2,1)} async-done(((bf16[1024,2048]{1,0:T(8,128)(2,1)}), bf16[1024,1024]{1,0:T(8,128)(2,1)}) %reduce-scatter.5.cloned.1.call-update) | async-done | bytes 2097168 | tf_op jit(solution)/shard_map/reduce_scatter | solution.py:158
  676.9 2.1 fusion.42
  678.9 2.5 psum.15
  681.4 3.7 fusion.45
  (237 shorter events, 110.3 us)
Async XLA Ops:
  6.5 117.1 %copy-start = (bf16[2048,16]{0,1:T(8,128)(2,1)S(1)}, bf16[2048,16]{0,1:T(8,128)(2,1)}, u32[]{:S(2)}) copy-start(bf16[2048,16]{0,1:T(8,128)(2,1)} %param.23) | copy-start | bytes 196612
  6.5 22.0 %copy-start.12 = (f32[2048]{0:T(1024)S(1)}, f32[2048]{0:T(1024)}, u32[]{:S(2)}) copy-start(f32[2048]{0:T(1024)} %param.19) | copy-start | bytes 24580
  6.5 18.8 %all-gather.8.cloned.1.call-start = ((), (), s32[]{:S(2)}) async-start(), calls=%async_computation.2 | async-start | bytes 6291456 | tf_op jit(solution)/shard_map/all_gather | solution.py:96
  7.3 70.5 %all-gather.12.cloned.1.call-start = ((), (), s32[]{:S(2)}) async-start(), calls=%async_computation.4 | async-start | bytes 2359296 | tf_op jit(solution)/shard_map/all_gather | solution.py:108
  8.0 110.7 %all-gather.10.cloned.1.call-start = ((), (), s32[]{:S(2)}) async-start(), calls=%async_computation.3 | async-start | bytes 1179648 | tf_op jit(solution)/shard_map/all_gather | solution.py:106
  8.7 151.0 %all-gather.14.cloned.1.call-start = ((), (), s32[]{:S(2)}) async-start(), calls=%async_computation.5 | async-start | bytes 1179648 | tf_op jit(solution)/shard_map/all_gather | solution.py:105
  9.3 306.7 %all-gather.16.cloned.1.call-start = ((), (), s32[]{:S(2)}) async-start(), calls=%async_computation.6 | async-start | bytes 2359296 | tf_op jit(solution)/shard_map/all_gather | solution.py:142
  9.9 322.7 %reduce-scatter.3.cloned.1.call-start = ((), (), s32[]{:S(2)}) async-start(), calls=%async_computation.7 | async-start | bytes 6291456 | tf_op jit(solution)/shard_map/reduce_scatter | solution.py:143
  25.3 3.4 copy-start.3
  84.5 39.1 %copy-start.16 = (bf16[16,256]{1,0:T(8,128)(2,1)S(1)}, bf16[16,256]{1,0:T(8,128)(2,1)}, u32[]{:S(2)}) copy-start(bf16[16,256]{1,0:T(8,128)(2,1)} %param.24) | copy-start | bytes 24580
  84.5 39.1 %copy-start.18 = (f32[1024,1]{0,1:T(1,128)S(1)}, f32[1024,1]{0,1:T(1,128)}, u32[]{:S(2)}) copy-start(f32[1024,1]{0,1:T(1,128)} %param.26) | copy-start | bytes 12292
  84.5 39.1 %copy-start.19 = (f32[256]{0:T(256)S(1)}, f32[256]{0:T(256)}, u32[]{:S(2)}) copy-start(f32[256]{0:T(256)} %param.25) | copy-start | bytes 3076
  164.5 151.2 %copy-start.15 = (f32[512]{0:T(512)S(1)}, f32[512]{0:T(512)}, u32[]{:S(2)}) copy-start(f32[512]{0:T(512)} %param.27) | copy-start | bytes 6148
  321.9 15.3 %copy-start.4 = (bf16[1024,1024]{1,0:T(8,128)(2,1)S(1)}, bf16[1024,1024]{1,0:T(8,128)(2,1)}, u32[]{:S(2)}) copy-start(bf16[1024,1024]{1,0:T(8,128)(2,1)} %param.18) | copy-start | bytes 6291460
  321.9 15.3 %copy-start.13 = (f32[1024]{0:T(1024)S(1)}, f32[1024]{0:T(1024)}, u32[]{:S(2)}) copy-start(f32[1024]{0:T(1024)} %param.29) | copy-start | bytes 12292
  321.9 313.6 %all-gather.18.cloned.1.call-start = ((), (), s32[]{:S(2)}) async-start(), calls=%async_computation.8 | async-start | bytes 6291456 | tf_op jit(solution)/shard_map/all_gather | solution.py:151
  337.2 4.6 copy-start.5
  341.0 297.6 %all-gather.20.cloned.1.call-start = ((), (), s32[]{:S(2)}) async-start(), calls=%async_computation.9 | async-start | bytes 9437184 | tf_op jit(solution)/shard_map/all_gather | solution.py:157
  341.8 335.1 %reduce-scatter.5.cloned.1.call-start = ((), (), s32[]{:S(2)}) async-start(), calls=%async_computation.10 | async-start | bytes 6291456 | tf_op jit(solution)/shard_map/reduce_scatter | solution.py:158
  341.8 28.2 %collective-permute-start = (bf16[256,2048]{1,0:T(8,128)(2,1)S(1)}, bf16[256,2048]{1,0:T(8,128)(2,1)S(1)}, u32[]{:S(2)}, u32[]{:S(2)}) collective-permute-start(bf16[256,2048]{1,0:T(8,128)(2,1)S(1)} %copy-done.5), channel_id=1, source_target_pairs={{0,2},{2,4},{4,6},{6,8},{8,10},{10,12},{12,14},{14,0},{1,3},{3,5},... | collective-permute-start | bytes 3145736 | tf_op jit(solution)/shard_map/ppermute | solution.py:17
  370.0 48.4 %collective-permute-start.1 = (bf16[256,2048]{1,0:T(8,128)(2,1)S(1)}, bf16[256,2048]{1,0:T(8,128)(2,1)S(1)}, u32[]{:S(2)}, u32[]{:S(2)}) collective-permute-start(bf16[256,2048]{1,0:T(8,128)(2,1)S(1)} %collective-permute-done), channel_id=1, source_target_pairs={{0,2},{2,4},{4,6},{6,8},{8,10},{10,12},{12,14},{14,0},{1,3},{3,5},... | collective-permute-start | bytes 3145736 | tf_op jit(solution)/shard_map/ppermute | solution.py:17
  418.4 42.5 %collective-permute-start.2 = (bf16[256,2048]{1,0:T(8,128)(2,1)S(1)}, bf16[256,2048]{1,0:T(8,128)(2,1)S(1)}, u32[]{:S(2)}, u32[]{:S(2)}) collective-permute-start(bf16[256,2048]{1,0:T(8,128)(2,1)S(1)} %collective-permute-done.1), channel_id=1, source_target_pairs={{0,2},{2,4},{4,6},{6,8},{8,10},{10,12},{12,14},{14,0},{1,3},{3,5},... | collective-permute-start | bytes 3145736 | tf_op jit(solution)/shard_map/ppermute | solution.py:17
  460.9 1.0 copy-start.6
  461.9 50.2 %collective-permute-start.3 = (bf16[256,2048]{1,0:T(8,128)(2,1)S(1)}, bf16[256,2048]{1,0:T(8,128)(2,1)S(1)}, u32[]{:S(2)}, u32[]{:S(2)}) collective-permute-start(bf16[256,2048]{1,0:T(8,128)(2,1)S(1)} %collective-permute-done.2), channel_id=1, source_target_pairs={{0,2},{2,4},{4,6},{6,8},{8,10},{10,12},{12,14},{14,0},{1,3},{3,5},... | collective-permute-start | bytes 3145736 | tf_op jit(solution)/shard_map/ppermute | solution.py:17
  512.0 1.0 copy-start.8
  513.0 49.9 %collective-permute-start.4 = (bf16[256,2048]{1,0:T(8,128)(2,1)S(1)}, bf16[256,2048]{1,0:T(8,128)(2,1)S(1)}, u32[]{:S(2)}, u32[]{:S(2)}) collective-permute-start(bf16[256,2048]{1,0:T(8,128)(2,1)S(1)} %collective-permute-done.3), channel_id=1, source_target_pairs={{0,2},{2,4},{4,6},{6,8},{8,10},{10,12},{12,14},{14,0},{1,3},{3,5},... | collective-permute-start | bytes 3145736 | tf_op jit(solution)/shard_map/ppermute | solution.py:17
  563.0 1.0 copy-start.10
  564.0 24.2 %collective-permute-start.5 = (bf16[256,2048]{1,0:T(8,128)(2,1)S(1)}, bf16[256,2048]{1,0:T(8,128)(2,1)}, u32[]{:S(2)}, u32[]{:S(2)}) collective-permute-start(bf16[256,2048]{1,0:T(8,128)(2,1)S(1)} %collective-permute-done.4), channel_id=1, source_target_pairs={{0,2},{2,4},{4,6},{6,8},{8,10},{10,12},{12,14},{14,0},{1,3},{3,5},... | collective-permute-start | bytes 3145736 | tf_op jit(solution)/shard_map/ppermute | solution.py:17
  588.2 25.2 %collective-permute-start.6 = (bf16[256,2048]{1,0:T(8,128)(2,1)}, bf16[256,2048]{1,0:T(8,128)(2,1)}, u32[]{:S(2)}, u32[]{:S(2)}) collective-permute-start(bf16[256,2048]{1,0:T(8,128)(2,1)} %collective-permute-done.5), channel_id=1, source_target_pairs={{0,2},{2,4},{4,6},{6,8},{8,10},{10,12},{12,14},{14,0},{1,3},{3,5},... | collective-permute-start | bytes 3145736 | tf_op jit(solution)/shard_map/ppermute | solution.py:17
  588.2 29.9 %copy-start.11 = (bf16[256,2048]{1,0:T(8,128)(2,1)S(1)}, bf16[256,2048]{1,0:T(8,128)(2,1)}, u32[]{:S(2)}) copy-start(bf16[256,2048]{1,0:T(8,128)(2,1)} %copy-done.10) | copy-start | bytes 3145732
  588.2 30.9 %copy-start.9 = (bf16[256,2048]{1,0:T(8,128)(2,1)S(1)}, bf16[256,2048]{1,0:T(8,128)(2,1)}, u32[]{:S(2)}) copy-start(bf16[256,2048]{1,0:T(8,128)(2,1)} %copy-done.8) | copy-start | bytes 3145732
  588.2 31.9 %copy-start.7 = (bf16[256,2048]{1,0:T(8,128)(2,1)S(1)}, bf16[256,2048]{1,0:T(8,128)(2,1)}, u32[]{:S(2)}) copy-start(bf16[256,2048]{1,0:T(8,128)(2,1)} %copy-done.6) | copy-start | bytes 3145732
  633.4 5.2 copy-start.17
  664.5 17.0 %copy-start.2 = (bf16[1024,1024]{1,0:T(8,128)(2,1)S(1)}, bf16[1024,1024]{1,0:T(8,128)(2,1)}, u32[]{:S(2)}) copy-start(bf16[1024,1024]{1,0:T(8,128)(2,1)} %fusion.41) | copy-start | bytes 6291460
  664.5 17.0 %copy-start.14 = (f32[1024]{0:T(1024)S(1)}, f32[1024]{0:T(1024)}, u32[]{:S(2)}) copy-start(f32[1024]{0:T(1024)} %param.33) | copy-start | bytes 12292
  664.5 20.7 %copy-start.1 = (bf16[2048,16]{0,1:T(8,128)(2,1)S(1)}, bf16[2048,16]{0,1:T(8,128)(2,1)}, u32[]{:S(2)}) copy-start(bf16[2048,16]{0,1:T(8,128)(2,1)} %param.23) | copy-start | bytes 196612
Sparse Core Ops, SparseCore 0:
  8.9 16.3 all-gather.7
  27.4 50.2 all-gather.11
  79.8 38.7 all-gather.9
  120.7 38.9 all-gather.13
  161.6 49.1 all-gather.15
  322.0 10.5 reduce-scatter.2
  341.2 14.9 all-gather.17
  358.2 189.4 all-gather.19
  664.6 12.2 reduce-scatter.4
